TPU v7x, 32 devices: a whole 2x2x4 slice. The times are simulated.
32 devices in a mesh: sp: 8 (over z, x), dp: 4 (over y, core).
Axes of the slice: x: 2, y: 2, z: 4, core: 2. Of those that a mesh axis runs over, the one named last changes fastest.
Arguments:
- tokens: bfloat16 [32, 512, 2048], P('dp', 'sp'), may hold values from -6 to 6
- pre_gain: float32 [2048], replicated, may hold values from 0.1 to 1.9
- w_query: bfloat16 [2048, 512], P('dp'), may hold values from -0.125 to 0.125
- w_forget: bfloat16 [2048, 512], P('dp'), may hold values from -0.125 to 0.125
- w_value: bfloat16 [2048, 512], P('dp'), may hold values from -0.125 to 0.125
- w_gate: bfloat16 [2048, 512], P('dp'), may hold values from -0.125 to 0.125
- lower_bound: float32 [512], replicated, may hold values from 0.8 to 1
- extra_decay: float32 [128, 512], P(('dp', 'sp')), may hold values from -1.5 to 0
- initial_state: float32 [128, 128, 128], P(('dp', 'sp')), may hold values from -0.18 to 0.18
- norm_gain: float32 [128], replicated, may hold values from 0.1 to 1.9
- w_out: bfloat16 [512, 2048], P('dp'), may hold values from -0.25 to 0.25
- post_gain: float32 [2048], replicated, may hold values from 0.1 to 1.9
Outputs:
- layer_out: bfloat16 [32, 512, 2048], P('dp', 'sp')
All inputs are finite; a program needn't handle non-finite values.
Results may differ from a plain program's by a relative error of at most 0.015.
Values may be sent and summed in bfloat16 or wider, within the bound.
A program may use at most 64 MiB of HBM per device.

v0:
```python
import functools

import jax
import jax.numpy as jnp
from jax import lax
from jax.experimental import pallas as pl
from jax.experimental.pallas import tpu as pltpu
from jax.sharding import PartitionSpec as P

EPS = 1e-06
MESH = pl.DeviceIdType.MESH


def rms_scale(matrix, gain):
    widened = matrix.astype(jnp.float32)
    return widened * lax.rsqrt(jnp.mean(widened * widened, axis=-1, keepdims=True) + EPS) * gain


def layer_kernel(
    n,
    ways,
    heads,
    tokens_hbm,
    pre_hbm,
    w0,
    w1,
    w2,
    w3,
    w4,
    extra_hbm,
    bound_hbm,
    init_hbm,
    gain_hbm,
    out_ref,
    a4,
    a0,
    a1,
    a2,
    a3,
    tokens_ref,
    pre_ref,
    raw_ref,
    extra_ref,
    bound_ref,
    start_ref,
    init_ref,
    gain_ref,
    normed,
    f_v_ref,
    q_g_ref,
    cum_ref,
    keys_ref,
    rbuf,
    sbuf,
    send_sem,
    recv_sem,
    init_sem,
    y_send,
    y_recv,
    x_send,
    x_recv,
    s_send,
    s_recv,
    local_sem,
    e_send,
    e_recv,
):
    me = lax.axis_index("sp")
    rank = lax.axis_index("dp")
    items, hv, hk = rbuf.shape
    own = init_ref.shape[0]
    seqs, length, width = tokens_ref.shape
    cols = heads * hk
    tile = 2 * hk
    shards = (w0, w1, w2, w3, w4)
    wholes = (a0, a1, a2, a3, a4)
    side = lax.rem(me, 2)
    beside = me + 1 - 2 * side
    sibling = rank + 1 - 2 * lax.rem(rank, 2)
    peers = ways // 2 - 1

    def local_copy(w):
        return pltpu.make_async_copy(shards[w], full(w, rank), local_sem.at[w])

    def full(w, shard):
        rows = shards[w].shape[0]
        return wholes[w].at[pl.ds(pl.multiple_of(shard * rows, rows), rows)]

    small = [
        pltpu.make_async_copy(src, dst, local_sem.at[5 + j])
        for j, (src, dst) in enumerate(
            (
                (tokens_hbm, tokens_ref),
                (pre_hbm, pre_ref),
                (extra_hbm, raw_ref.at[me]),
                (bound_hbm, bound_ref),
                (init_hbm, start_ref),
                (gain_hbm, gain_ref),
            )
        )
    ]
    for w in range(5):
        local_copy(w).start()
    for copy in small:
        copy.start()

    barrier = pltpu.get_barrier_semaphore()
    for offset in range(1, n):
        pl.semaphore_signal(
            barrier, inc=1, device_id={"sp": lax.rem(me + offset, n)}, device_id_type=MESH
        )
    for offset in range(1, ways):
        pl.semaphore_signal(
            barrier, inc=1, device_id={"dp": lax.rem(rank + offset, ways)}, device_id_type=MESH
        )
    pl.semaphore_wait(barrier, n + ways - 2)

    def part(w, shard, half):
        rows = shards[w].shape[0]
        start = shard * rows + half * (rows // 2)
        return wholes[w].at[pl.ds(pl.multiple_of(start, rows // 2), rows // 2)]

    def remote(src, dst, send, recv, device):
        return pltpu.make_async_remote_copy(
            src_ref=src,
            dst_ref=dst,
            send_sem=send,
            recv_sem=recv,
            device_id=device,
            device_id_type=MESH,
        )

    def y_copy(w, k):
        ref = part(w, rank, side)
        target = lax.rem(rank + 2 * (k + 1), ways)
        return remote(ref, ref, y_send.at[w, k], y_recv.at[w, k], {"dp": target})

    def origin(k):
        return lax.rem(rank + ways - 2 * (k + 1), ways)

    def x_copy(w, k):
        ref = part(w, origin(k), side)
        return remote(ref, ref, x_send.at[w, k], x_recv.at[w, k], {"sp": beside})

    def s_own(w):
        ref = full(w, rank)
        return remote(ref, ref, s_send.at[w, 0], s_recv.at[w, 0], {"dp": sibling})

    def s_copy(w, k, second):
        ref = part(w, origin(k), 1 - side if second else side)
        slot = 1 + 2 * k + second
        return remote(ref, ref, s_send.at[w, slot], s_recv.at[w, slot], {"dp": sibling})

    def pass_y(w):
        for k in range(peers):
            y_copy(w, k).wait_recv()
            x_copy(w, k).start()
            s_copy(w, k, 0).start()

    def pass_x(w):
        for k in range(peers):
            x_copy(w, k).wait_recv()
            s_copy(w, k, 1).start()

    def arrived(w):
        s_own(w).wait_recv()
        for k in range(peers):
            s_copy(w, k, 0).wait_recv()
            s_copy(w, k, 1).wait_recv()

    def init_copy(j):
        return remote(
            init_ref.at[j],
            rbuf.at[me * own + j],
            init_sem.at[j],
            recv_sem.at[me * own + j],
            {"sp": 0},
        )

    def chain_copy(it):
        return remote(
            sbuf.at[it],
            rbuf.at[it],
            send_sem.at[it],
            recv_sem.at[it],
            {"sp": lax.rem(me + 1, n)},
        )

    def extra_copy(offset):
        return remote(
            raw_ref.at[me],
            raw_ref.at[me],
            e_send.at[offset - 1],
            e_recv.at[offset - 1],
            {"sp": lax.rem(me + offset, n)},
        )

    for w in range(5):
        local_copy(w).wait()
        for k in range(peers):
            y_copy(w, k).start()
        s_own(w).start()
    for copy in small:
        copy.wait()
    for offset in range(1, n):
        extra_copy(offset).start()
    for j in range(own):
        init_ref[j] = start_ref[j].T.astype(jnp.bfloat16)

    def norm_rows(s, carry):
        rows = pl.ds(pl.multiple_of(s * length, length), length)
        normed[rows, :] = rms_scale(tokens_ref[s], pre_ref[...]).astype(jnp.bfloat16)
        return carry

    lax.fori_loop(0, seqs, norm_rows, 0)

    @pl.when(me > 0)
    def _():
        for j in range(own):
            init_copy(j).start()

    @pl.when(me == 0)
    def _():
        rbuf[0:own] = init_ref[...]

    gap = 1.0 - bound_ref[...]
    row = lax.broadcasted_iota(jnp.int32, (length, length), 0)
    col = lax.broadcasted_iota(jnp.int32, (length, length), 1)
    causal = row >= col
    ones = causal.astype(jnp.float32)
    nt = (((1,), (1,)), ((), ()))
    tn = (((0,), (0,)), ((), ()))
    place = (length, n * length)
    chosen = (
        lax.broadcasted_iota(jnp.int32, place, 1)
        == lax.broadcasted_iota(jnp.int32, place, 0) + me * length
    ).astype(jnp.float32)
    for offset in range(1, n):
        extra_copy(offset).wait_recv()

    def pick(i, carry):
        extra_ref[i] = lax.dot_general(
            chosen,
            raw_ref[i],
            nt,
            precision=lax.Precision.HIGHEST,
            preferred_element_type=jnp.float32,
        )
        return carry

    lax.fori_loop(0, n, pick, 0)

    def project(w, dest, at, j):
        lanes = pl.ds(pl.multiple_of(j * tile, tile), tile)
        where = pl.ds(pl.multiple_of(at + j * tile, tile), tile)
        dest[:, where] = jnp.dot(
            normed[...], wholes[w][:, lanes], preferred_element_type=jnp.float32
        ).astype(jnp.bfloat16)

    def project_all(w, dest, at):
        def step(j, carry):
            project(w, dest, at, j)
            return carry

        lax.fori_loop(0, cols // tile, step, 0)

    pass_y(0)
    pass_y(1)
    pass_x(0)
    arrived(0)
    project_all(0, f_v_ref, 0)
    pass_x(1)
    pass_y(2)
    arrived(1)
    project_all(1, f_v_ref, cols)
    tiles = cols // tile

    def forward(s, carry):
        rows = pl.ds(pl.multiple_of(s * length, length), length)
        f_pre = f_v_ref[rows, 0:cols].astype(jnp.float32)
        keys = gap * jax.nn.sigmoid(-f_pre)
        spread = jnp.concatenate(
            [
                jnp.broadcast_to(
                    extra_ref[s * (heads // own) + h // own][:, h % own : h % own + 1],
                    (length, hk),
                )
                for h in range(heads)
            ],
            axis=1,
        )
        decay = jnp.log1p(-keys) + spread
        cum = jnp.dot(
            ones, decay, precision=lax.Precision.HIGHEST, preferred_element_type=jnp.float32
        )
        end = cum[length - 1 : length, :]
        mid = cum[length // 2 : length // 2 + 1, :]
        keys_end = (keys * jnp.exp(end - cum)).astype(jnp.bfloat16)
        keys_ref[rows, :] = (keys * jnp.exp(mid - cum)).astype(jnp.bfloat16)
        cum_ref[rows, :] = cum
        end_decay = jnp.exp(end)
        added = []
        for h in range(heads):
            lanes = slice(h * hk, (h + 1) * hk)
            values = f_v_ref[rows, cols + h * hv : cols + (h + 1) * hv]
            added.append(
                lax.dot_general(
                    values, keys_end[:, lanes], tn, preferred_element_type=jnp.float32
                )
            )
        for h in range(heads):
            lanes = slice(h * hk, (h + 1) * hk)
            it = s * heads + h

            @pl.when(jnp.logical_or(me > 0, it >= own))
            def _():
                chain_copy(it).wait_recv()

            @pl.when(me < n - 1)
            def _():
                state = rbuf[it].astype(jnp.float32)
                sbuf[it] = (state * end_decay[:, lanes] + added[h]).astype(jnp.bfloat16)
                chain_copy(it).start()

        @pl.when(s == 0)
        def _():
            pass_x(2)
            pass_y(3)

        @pl.when(s == tiles)
        def _():
            arrived(2)

        @pl.when(s == 2 * tiles - 1)
        def _():
            pass_x(3)
            pass_y(4)

        @pl.when(s == 2 * tiles)
        def _():
            arrived(3)

        @pl.when(s == 3 * tiles)
        def _():
            pass_x(4)

        @pl.when(jnp.logical_and(s >= tiles, s < 2 * tiles))
        def _():
            project(2, q_g_ref, 0, s - tiles)

        @pl.when(jnp.logical_and(s >= 2 * tiles, s < 3 * tiles))
        def _():
            project(3, q_g_ref, cols, s - 2 * tiles)

        return carry

    lax.fori_loop(0, seqs, forward, 0)

    def outputs(s, carry):
        rows = pl.ds(pl.multiple_of(s * length, length), length)
        cum = cum_ref[rows, :]
        mid = cum[length // 2 : length // 2 + 1, :]
        q_pre = q_g_ref[rows, 0:cols].astype(jnp.float32)
        queries = q_pre * jax.nn.sigmoid(q_pre)
        q_carry = (queries * jnp.exp(cum)).astype(jnp.bfloat16)
        q_mid = (queries * jnp.exp(cum - mid)).astype(jnp.bfloat16)
        for h in range(heads):
            lanes = slice(h * hk, (h + 1) * hk)
            it = s * heads + h
            values = f_v_ref[rows, cols + h * hv : cols + (h + 1) * hv]
            scores = lax.dot_general(
                q_mid[:, lanes], keys_ref[rows, lanes], nt, preferred_element_type=jnp.float32
            )
            scores = jnp.where(causal, scores, 0.0).astype(jnp.bfloat16)
            outs = jnp.dot(scores, values, preferred_element_type=jnp.float32) + lax.dot_general(
                q_carry[:, lanes], rbuf[it], nt, preferred_element_type=jnp.float32
            )
            scaled = rms_scale(outs, gain_ref[...]).astype(jnp.bfloat16).astype(jnp.float32)
            g_pre = q_g_ref[rows, cols + h * hv : cols + (h + 1) * hv].astype(jnp.float32)
            out_ref[rows, h * hv : (h + 1) * hv] = (
                scaled * (g_pre * jax.nn.sigmoid(g_pre))
            ).astype(jnp.bfloat16)
        return carry

    lax.fori_loop(0, seqs, outputs, 0)
    arrived(4)
    for offset in range(1, n):
        extra_copy(offset).wait_send()
    for w in range(5):
        s_own(w).wait_send()
        for k in range(peers):
            y_copy(w, k).wait_send()
            x_copy(w, k).wait_send()
            s_copy(w, k, 0).wait_send()
            s_copy(w, k, 1).wait_send()

    @pl.when(me > 0)
    def _():
        for j in range(own):
            init_copy(j).wait_send()

    @pl.when(me < n - 1)
    def _():
        def done(it, carry):
            chain_copy(it).wait_send()
            return carry

        lax.fori_loop(0, items, done, 0)


def layer(tokens, pre, weights, extra, bound, init, gain, n, ways):
    own, hk, hv = init.shape
    seqs, length, width = tokens.shape
    items = own * n
    heads = items // seqs
    rows = seqs * length
    peers = max(ways // 2 - 1, 1)
    vmem = pl.BlockSpec(memory_space=pltpu.VMEM)
    dma = pltpu.SemaphoreType.DMA

    def whole(w):
        return (w.shape[0] * ways, w.shape[1])

    return pl.pallas_call(
        functools.partial(layer_kernel, n, ways, heads),
        out_shape=[
            jax.ShapeDtypeStruct((rows, heads * hv), jnp.bfloat16),
            jax.ShapeDtypeStruct(whole(weights[4]), jnp.bfloat16),
        ],
        in_specs=[pl.BlockSpec(memory_space=pltpu.HBM)] * 11,
        out_specs=[vmem] * 2,
        scratch_shapes=[pltpu.VMEM(whole(w), jnp.bfloat16) for w in weights[:4]]
        + [
            pltpu.VMEM(tokens.shape, jnp.bfloat16),
            pltpu.VMEM(pre.shape, jnp.float32),
            pltpu.VMEM((n,) + extra.shape, jnp.float32),
            pltpu.VMEM((n, length, own), jnp.float32),
            pltpu.VMEM(bound.shape, jnp.float32),
            pltpu.VMEM(init.shape, jnp.float32),
            pltpu.VMEM((own, hv, hk), jnp.bfloat16),
            pltpu.VMEM(gain.shape, jnp.float32),
            pltpu.VMEM((rows, width), jnp.bfloat16),
            pltpu.VMEM((rows, heads * (hk + hv)), jnp.bfloat16),
            pltpu.VMEM((rows, heads * (hk + hv)), jnp.bfloat16),
            pltpu.VMEM((rows, heads * hk), jnp.float32),
            pltpu.VMEM((rows, heads * hk), jnp.bfloat16),
            pltpu.VMEM((items, hv, hk), jnp.bfloat16),
            pltpu.VMEM((items, hv, hk), jnp.bfloat16),
            dma((items,)),
            dma((items,)),
            dma((own,)),
            dma((5, peers)),
            dma((5, peers)),
            dma((5, peers)),
            dma((5, peers)),
            dma((5, 1 + 2 * peers)),
            dma((5, 1 + 2 * peers)),
            dma((11,)),
            dma((n - 1,)),
            dma((n - 1,)),
        ],
        compiler_params=pltpu.CompilerParams(
            collective_id=0, has_side_effects=True, vmem_limit_bytes=48 * 1024 * 1024
        ),
        cost_estimate=pl.CostEstimate(
            flops=6 * 10**9, bytes_accessed=2 * 10**7, transcendentals=10**6
        ),
    )(tokens, pre, *weights, extra, bound, init, gain)


def body(
    n,
    ways,
    tokens,
    pre_gain,
    w_query,
    w_forget,
    w_value,
    w_gate,
    lower_bound,
    extra_decay,
    initial_state,
    norm_gain,
    w_out,
    post_gain,
):
    seq_count, local_len, width = tokens.shape
    gated, w_o = layer(
        tokens,
        pre_gain[None, :],
        (w_forget, w_value, w_query, w_gate, w_out),
        extra_decay,
        lower_bound[None, :],
        initial_state,
        norm_gain[None, :],
        n,
        ways,
    )
    mixed = jnp.dot(gated, w_o, preferred_element_type=jnp.float32)
    return rms_scale(mixed, post_gain).astype(jnp.bfloat16).reshape(seq_count, local_len, width)


def solution(mesh):
    in_specs = (
        P("dp", "sp", None),
        P(),
        P("dp", None),
        P("dp", None),
        P("dp", None),
        P("dp", None),
        P(),
        P(("dp", "sp"), None),
        P(("dp", "sp"), None, None),
        P(),
        P("dp", None),
        P(),
    )
    out_specs = P("dp", "sp", None)
    return jax.shard_map(
        functools.partial(body, mesh.shape["sp"], mesh.shape["dp"]),
        mesh=mesh,
        in_specs=in_specs,
        out_specs=out_specs,
        check_vma=False,
    )
```

profile of v0, /device:TPU:26, one launch (start us, length us, event | category | flops | bytes accessed | tf_op | source)
XLA Modules:
  0.0 110.4 jit_solution(15108138324984087710)
XLA Ops:
  0.0 0.0 copy-start
  0.0 1.0 copy-done
  1.0 0.0 copy-start.1
  1.0 1.0 copy-done.1
  2.1 0.0 copy-start.2
  2.1 1.0 copy-done.2
  3.1 0.0 copy-start.3
  3.1 1.0 copy-done.3
  4.2 0.0 copy-start.4
  4.2 1.0 copy-done.4
  5.2 0.0 copy-start.5
  5.2 0.9 copy-done.5
  6.2 0.0 copy-start.6
  6.2 0.7 copy-done.6
  6.9 0.0 copy-start.7
  6.9 0.7 copy-done.7
  7.6 0.0 copy-start.8
  7.6 0.7 copy-done.8
  8.2 0.0 copy-start.9
  8.2 0.7 copy-done.9
  8.9 98.3 %shard_map.118 = (bf16[512,512]{1,0:T(8,128)(2,1)S(1)}, bf16[512,2048]{1,0:T(8,128)(2,1)S(1)}) custom-call(bf16[8,64,2048]{2,1,0:T(8,128)(2,1)} %tokens_hbm.1, f32[1,2048]{1,0:T(1,128)S(1)} %bitcast.6, bf16[512,512]{1,0:T(8,128)(2,1)S(1)} %copy-done, bf16[512,512]{1,0:T(8,128)(2,1)S(1)} %copy-done.1, bf16[512,512]{1,0:T(8,128)(2,1)S(1)} %copy-done.2, ...), custom_call_target="tpu_custom_call" | custom-call | flops 6000000000 | bytes 20000000 | tf_op jit(solution)/shard_map/pallas_call | solution.py:424
  107.3 0.0 copy-start.10
  107.3 1.3 %multiply_reduce_fusion = (f32[512]{0:T(512)S(1)}, f32[512,2048]{1,0:T(8,128)S(1)}) fusion(bf16[512,512]{1,0:T(8,128)(2,1)S(1)} %get-tuple-element.7, bf16[512,2048]{1,0:T(8,128)(2,1)S(1)} %get-tuple-element.8), kind=kOutput, calls=%fused_computation.1 | convolution fusion | flops 1075838464 | bytes 6817792 | tf_op jit(solution)/shard_map/dot_general | solution.py:499
  108.6 0.0 copy-done.10
  108.6 1.7 %multiply_convert_fusion = bf16[512,2048]{1,0:T(8,128)(2,1)} fusion(f32[512,2048]{1,0:T(8,128)S(1)} %get-tuple-element.10, f32[2048]{0:T(1024)S(1)} %copy-done.10, f32[512]{0:T(512)S(1)} %add_rsqrt_fusion), kind=kLoop, calls=%fused_computation | loop fusion | flops 3145728 | bytes 6301696 | tf_op jit(solution)/shard_map/convert_element_type | solution.py:500
  (1 shorter events, 0.0 us)
Async XLA Ops:
  0.0 1.0 copy-start
  1.0 1.0 copy-start.1
  2.1 1.0 copy-start.2
  3.1 1.0 copy-start.3
  4.2 1.0 copy-start.4
  5.2 0.9 copy-start.5
  6.2 0.7 copy-start.6
  6.9 0.7 copy-start.7
  7.6 0.7 copy-start.8
  8.2 0.7 copy-start.9
  107.3 1.4 %copy-start.10 = (f32[2048]{0:T(1024)S(1)}, f32[2048]{0:T(1024)}, u32[]{:S(2)}) copy-start(f32[2048]{0:T(1024)} %param.23) | copy-start | bytes 24580
where the time goes:
time: 111 us; the launch traced here: 110 us
  Pallas kernels  98.3 us (89%)
  local copies, waits for them, and re-layouts  8.89 us (8%)
  other arithmetic  1.74 us (2%)
  matrix products  1.35 us (1%)
    pallas_call x1, Pallas kernels, layer(): pl.pallas_call(functools.partial(layer_kernel, n, ways, heads), out_shape...  98.3 us
    unnamed x22, local copies, waits for them, and re-layouts  8.89 us

commit v1 on v0

v1 whole, which is shorter than its diff:
```python
import functools

import jax
import jax.numpy as jnp
from jax import lax
from jax.experimental import pallas as pl
from jax.experimental.pallas import tpu as pltpu
from jax.sharding import PartitionSpec as P

EPS = 1e-06
MESH = pl.DeviceIdType.MESH
NT = (((1,), (1,)), ((), ()))
TN = (((0,), (0,)), ((), ()))


def rms_scale(matrix, gain):
    widened = matrix.astype(jnp.float32)
    return widened * lax.rsqrt(jnp.mean(widened * widened, axis=-1, keepdims=True) + EPS) * gain


def layer_kernel(
    n,
    ways,
    heads,
    axes,
    tokens_hbm,
    pre_hbm,
    wf_hbm,
    wv_hbm,
    wq_hbm,
    wg_hbm,
    wo_hbm,
    extra_hbm,
    bound_hbm,
    init_hbm,
    gain_hbm,
    post_hbm,
    out_ref,
    *scratch,
):
    units = len(axes)
    groups = heads // 2
    wholes = scratch[:units]
    (
        tokens_ref,
        pre_ref,
        raw_ref,
        bound_ref,
        start_ref,
        gain_ref,
        post_ref,
        normed,
        f_ref,
        v_ref,
        q_ref,
        g_ref,
        keys_ref,
        rel_ref,
        emid_ref,
        eend_ref,
        within_ref,
        gated_ref,
        mixed_ref,
        esend,
        erecv,
        extra_ref,
        isend,
        st,
        fin,
        bb,
        bs,
        ob,
        dbuf,
        dsend,
        local_sem,
        y_send,
        y_recv,
        r_send,
        r_recv,
        s_send,
        s_recv,
        e_send,
        e_recv,
        i_send,
        b_send,
        b_recv,
        d_send,
        d_recv,
        c_send,
        c_recv,
        t_send,
        t_recv,
    ) = scratch[units:]
    me = lax.axis_index("sp")
    rank = lax.axis_index("dp")
    seqs, length, width = tokens_ref.shape
    own, hk, hv = start_ref.shape
    half = 2 * hk
    cols = heads * hk
    total = groups * seqs
    levels = n // 2
    side = lax.rem(me, 2)
    level = me // 2
    parity = lax.rem(level, 2)
    beside = me + 1 - 2 * side
    across = me + 2 - 4 * parity
    sibling = rank + 1 - 2 * lax.rem(rank, 2)
    peers = ways // 2 - 1
    unit_q, unit_g, unit_o = 2 * groups, 2 * groups + 1, 2 * groups + 2

    def source(u):
        if u < 2 * groups:
            base = wf_hbm if u % 2 == 0 else wv_hbm
            return base.at[:, (u // 2) * half : (u // 2 + 1) * half]
        return (wq_hbm, wg_hbm, wo_hbm)[u - 2 * groups]

    def full(u, shard):
        rows = wholes[u].shape[0] // ways
        return wholes[u].at[pl.ds(pl.multiple_of(shard * rows, rows), rows)]

    def part(u, shard, which):
        rows = wholes[u].shape[0] // ways
        start = shard * rows + which * (rows // 2)
        return wholes[u].at[pl.ds(pl.multiple_of(start, rows // 2), rows // 2)]

    def local_copy(u):
        return pltpu.make_async_copy(source(u), full(u, rank), local_sem.at[u])

    small = [
        pltpu.make_async_copy(src, dst, local_sem.at[units + j])
        for j, (src, dst) in enumerate(
            (
                (extra_hbm, raw_ref),
                (init_hbm, start_ref),
                (tokens_hbm, tokens_ref),
                (pre_hbm, pre_ref),
                (bound_hbm, bound_ref),
                (gain_hbm, gain_ref),
                (post_hbm, post_ref),
            )
        )
    ]
    local_copy(0).start()
    for copy in small:
        copy.start()
    for u in range(1, units):
        local_copy(u).start()

    barrier = pltpu.get_barrier_semaphore()
    for offset in range(1, n):
        pl.semaphore_signal(
            barrier, inc=1, device_id={"sp": lax.rem(me + offset, n)}, device_id_type=MESH
        )
    for offset in range(1, ways):
        pl.semaphore_signal(
            barrier, inc=1, device_id={"dp": lax.rem(rank + offset, ways)}, device_id_type=MESH
        )
    pl.semaphore_wait(barrier, n + ways - 2)

    def remote(src, dst, send, recv, device):
        return pltpu.make_async_remote_copy(
            src_ref=src,
            dst_ref=dst,
            send_sem=send,
            recv_sem=recv,
            device_id=device,
            device_id_type=MESH,
        )

    def which(u):
        return side if axes[u] == "x" else parity

    def first_part(u, shard):
        return full(u, shard) if axes[u] is None else part(u, shard, which(u))

    def y_copy(u, k):
        ref = first_part(u, rank)
        target = lax.rem(rank + 2 * (k + 1), ways)
        return remote(ref, ref, y_send.at[u, k], y_recv.at[u, k], {"dp": target})

    def origin(k):
        return lax.rem(rank + ways - 2 * (k + 1), ways)

    def r_copy(u, k):
        ref = part(u, origin(k), which(u))
        device = {"sp": beside if axes[u] == "x" else across}
        return remote(ref, ref, r_send.at[u, k], r_recv.at[u, k], device)

    def s_own(u):
        ref = full(u, rank)
        return remote(ref, ref, s_send.at[u, 0], s_recv.at[u, 0], {"dp": sibling})

    def s_copy(u, k, second):
        ref = part(u, origin(k), 1 - which(u)) if second else first_part(u, origin(k))
        slot = 1 + 2 * k + second
        return remote(ref, ref, s_send.at[u, slot], s_recv.at[u, slot], {"dp": sibling})

    def pass_y(u):
        for k in range(peers):
            y_copy(u, k).wait_recv()
            if axes[u] is not None:
                r_copy(u, k).start()
            s_copy(u, k, 0).start()

    def pass_r(u):
        if axes[u] is None:
            return
        for k in range(peers):
            r_copy(u, k).wait_recv()
            s_copy(u, k, 1).start()

    def arrived(u):
        s_own(u).wait_recv()
        for k in range(peers):
            s_copy(u, k, 0).wait_recv()
            if axes[u] is not None:
                s_copy(u, k, 1).wait_recv()

    def e_copy(offset):
        target = lax.rem(me + offset, n)
        return remote(
            esend.at[target],
            erecv.at[me],
            e_send.at[offset - 1],
            e_recv.at[offset - 1],
            {"sp": target},
        )

    def place(j):
        it = me * own + j
        h = lax.rem(it, heads)
        return lax.rem(h, 2), (h // 2) * seqs + it // heads

    def i_copy(j):
        target, k = place(j)
        return remote(isend.at[j], st.at[k, 0], i_send.at[j], c_recv.at[k], {"sp": target})

    def b_copy(k):
        return remote(bs.at[k], bb.at[k, side], b_send.at[k], b_recv.at[k], {"sp": beside})

    def d_copy(g):
        return remote(dsend.at[g], dbuf.at[side, g], d_send.at[g], d_recv.at[g], {"sp": beside})

    def c_copy(k):
        target = lax.rem(me + 2, n)
        return remote(ob.at[k], st.at[k, 0], c_send.at[k], c_recv.at[k], {"sp": target})

    def t_copy(k):
        return remote(st.at[k, 1 - side], fin.at[k], t_send.at[k], t_recv.at[k], {"sp": beside})

    for u in range(units):
        local_copy(u).wait()
        for k in range(peers):
            y_copy(u, k).start()
        s_own(u).start()
    for copy in small:
        copy.wait()

    pad = esend.shape[2]
    for p in range(n):
        piece = raw_ref[:, p * length : (p + 1) * length]
        esend[p] = jnp.concatenate(
            [piece, jnp.zeros((own, pad - length), jnp.float32)], axis=1
        )
    for offset in range(1, n):
        e_copy(offset).start()
    for j in range(own):
        isend[j] = start_ref[j].T.astype(jnp.bfloat16)
    for j in range(own):
        target, k = place(j)

        @pl.when(me != target)
        def _():
            i_copy(j).start()

        @pl.when(me == target)
        def _():
            st[k, 0] = isend[j]

    def norm_rows(s, carry):
        rows = pl.ds(pl.multiple_of(s * length, length), length)
        normed[rows, :] = rms_scale(tokens_ref[s], pre_ref[...]).astype(jnp.bfloat16)
        return carry

    lax.fori_loop(0, seqs, norm_rows, 0)
    erecv[me] = esend[me]
    for offset in range(1, n):
        e_copy(offset).wait_recv()

    def turn(p, carry):
        extra_ref[p] = erecv[p].T
        return carry

    lax.fori_loop(0, n, turn, 0)

    gap = 1.0 - bound_ref[...]
    row = lax.broadcasted_iota(jnp.int32, (length, length), 0)
    col = lax.broadcasted_iota(jnp.int32, (length, length), 1)
    causal = row >= col
    ones = causal.astype(jnp.bfloat16)
    ones = jnp.concatenate([ones, ones], axis=1)
    middle = length // 2

    def seq_rows(s):
        return pl.ds(pl.multiple_of(s * length, length), length)

    def project(u, dest, at, tiles):
        def step(j, carry):
            lanes = pl.ds(pl.multiple_of(j * half, half), half)
            there = pl.ds(pl.multiple_of(at + j * half, half), half)
            dest[:, there] = jnp.dot(
                normed[...], wholes[u][:, lanes], preferred_element_type=jnp.float32
            ).astype(jnp.bfloat16)
            return carry

        lax.fori_loop(0, tiles, step, 0)

    def decays(g, s):
        rows = seq_rows(s)
        lanes = slice(g * half, (g + 1) * half)
        keys = gap[:, lanes] * jax.nn.sigmoid(-f_ref[rows, lanes].astype(jnp.float32))
        spread = jnp.concatenate(
            [
                jnp.broadcast_to(
                    extra_ref[s * (heads // own) + h // own][:length, h % own : h % own + 1],
                    (length, hk),
                )
                for h in (2 * g, 2 * g + 1)
            ],
            axis=1,
        )
        decay = jnp.log(1.0 - keys) + spread
        high = decay.astype(jnp.bfloat16)
        low = (decay - high.astype(jnp.float32)).astype(jnp.bfloat16)
        cum = jnp.dot(
            ones, jnp.concatenate([high, low], axis=0), preferred_element_type=jnp.float32
        )
        mid = cum[middle : middle + 1, :]
        end = cum[length - 1 : length, :]
        rel = cum - mid
        keys_ref[rows, lanes] = (keys * jnp.exp(-rel)).astype(jnp.bfloat16)
        rel_ref[rows, lanes] = rel
        emid_ref[pl.ds(s, 1), lanes] = jnp.exp(mid)
        eend_ref[pl.ds(s, 1), lanes] = jnp.exp(end - mid)
        both = jnp.exp(end)
        mine = jnp.where(side == 0, both[:, :hk], both[:, hk:])
        other = jnp.where(side == 0, both[:, hk:], both[:, :hk])
        dbuf[side, g, pl.ds(s, 1)] = mine
        dsend[g, pl.ds(s, 1)] = other

    def head_lanes(g, role):
        start = g * half + (side if role == 0 else 1 - side) * hk
        return pl.ds(pl.multiple_of(start, hk), hk)

    def added(g, s, role):
        rows = seq_rows(s)
        lanes = head_lanes(g, role)
        state = lax.dot_general(
            v_ref[rows, lanes], keys_ref[rows, lanes], TN, preferred_element_type=jnp.float32
        )
        ends = eend_ref[pl.ds(s, 1), g * half : (g + 1) * half]
        end = jnp.where(side == role, ends[:, :hk], ends[:, hk:])
        return (state * end).astype(jnp.bfloat16)

    def locals_of(g, s):
        k = g * seqs + s
        bs[k] = added(g, s, 1)
        b_copy(k).start()
        bb[k, side] = added(g, s, 0)

    def chain(k, carry):
        g = k // seqs
        s = lax.rem(k, seqs)
        holder = (s * heads + 2 * g + side) // own
        b_copy(k).wait_recv()

        @pl.when(jnp.logical_or(level > 0, holder != me))
        def _():
            c_copy(k).wait_recv()

        first = dbuf[0, g, pl.ds(s, 1)]
        between = st[k, 0].astype(jnp.float32) * first + bb[k, 0].astype(jnp.float32)
        st[k, 1] = between.astype(jnp.bfloat16)
        t_copy(k).start()

        @pl.when(level < levels - 1)
        def _():
            second = dbuf[1, g, pl.ds(s, 1)]
            ob[k] = (between * second + bb[k, 1].astype(jnp.float32)).astype(jnp.bfloat16)
            c_copy(k).start()

        return carry

    lag = 4

    def target(i):
        late = i + 1 - lag * level
        first = jnp.clip(late, 0, seqs)
        later = jnp.clip(late - 2 * seqs, 0, total - seqs)
        return first + later

    def chain_slot(i):
        lax.fori_loop(target(i - 1), target(i), chain, 0)

    def intra(s):
        rows = seq_rows(s)
        q_pre = q_ref[rows, :].astype(jnp.float32)
        q_mid = q_pre * jax.nn.sigmoid(q_pre) * jnp.exp(rel_ref[rows, :])
        q_near = q_mid.astype(jnp.bfloat16)
        q_ref[rows, :] = (q_mid * emid_ref[pl.ds(s, 1), :]).astype(jnp.bfloat16)
        for h in range(heads):
            lanes = slice(h * hk, (h + 1) * hk)
            scores = lax.dot_general(
                q_near[:, lanes], keys_ref[rows, lanes], NT, preferred_element_type=jnp.float32
            )
            scores = jnp.where(causal, scores, 0.0).astype(jnp.bfloat16)
            within_ref[rows, lanes] = jnp.dot(
                scores, v_ref[rows, lanes], preferred_element_type=jnp.float32
            )

    def finish(t, carry):
        for b in range(2):
            s = 2 * t + b
            rows = seq_rows(s)
            for g in range(groups):
                k = g * seqs + s
                for role in range(2):
                    lanes = head_lanes(g, role)
                    state = st[k, side] if role == 0 else fin[k]
                    outs = within_ref[rows, lanes] + lax.dot_general(
                        q_ref[rows, lanes], state, NT, preferred_element_type=jnp.float32
                    )
                    scaled = rms_scale(outs, gain_ref[...]).astype(jnp.bfloat16)
                    g_pre = g_ref[rows, lanes].astype(jnp.float32)
                    gated_ref[b * length : (b + 1) * length, lanes] = (
                        scaled.astype(jnp.float32) * (g_pre * jax.nn.sigmoid(g_pre))
                    ).astype(jnp.bfloat16)
        tile = 512
        squares = jnp.zeros((2 * length, 1), jnp.float32)
        for j in range(width // tile):
            lanes = slice(j * tile, (j + 1) * tile)
            mixed = jnp.dot(
                gated_ref[...], wholes[unit_o][:, lanes], preferred_element_type=jnp.float32
            )
            squares = squares + jnp.sum(mixed * mixed, axis=-1, keepdims=True)
            mixed_ref[:, lanes] = mixed
        scale = lax.rsqrt(squares * (1.0 / width) + EPS)
        rows = pl.ds(pl.multiple_of(t * 2 * length, 2 * length), 2 * length)
        for j in range(width // tile):
            lanes = slice(j * tile, (j + 1) * tile)
            out_ref[rows, lanes] = (mixed_ref[:, lanes] * scale * post_ref[:, lanes]).astype(
                jnp.bfloat16
            )
        return carry

    pass_y(0)
    pass_y(1)
    pass_r(0)
    arrived(0)
    project(0, f_ref, 0, 1)
    pass_y(2)

    def decay_first(s, carry):
        decays(0, s)

        @pl.when(s == seqs // 2)
        def _():
            pass_r(1)

        return carry

    lax.fori_loop(0, seqs, decay_first, 0)
    d_copy(0).start()
    pass_y(3)
    arrived(1)
    project(1, v_ref, 0, 1)

    def locals_first(s, carry):
        locals_of(0, s)
        return carry

    lax.fori_loop(0, seqs, locals_first, 0)
    pass_r(2)
    arrived(2)
    project(2, f_ref, half, 1)
    d_copy(0).wait_recv()

    def decay_later(s, carry):
        decays(1, s)
        chain_slot(s)

        @pl.when(s == seqs // 4)
        def _():
            pass_r(3)

        @pl.when(s == seqs // 2)
        def _():
            pass_y(unit_q)

        return carry

    lax.fori_loop(0, seqs, decay_later, 0)
    d_copy(1).start()
    arrived(3)
    project(3, v_ref, half, 1)

    def locals_later(s, carry):
        locals_of(1, s)
        chain_slot(seqs + s)

        @pl.when(s == seqs // 2)
        def _():
            pass_r(unit_q)

        return carry

    lax.fori_loop(0, seqs, locals_later, 0)
    pass_y(unit_g)
    d_copy(1).wait_recv()
    arrived(unit_q)
    project(unit_q, q_ref, 0, cols // half)

    def intra_later(s, carry):
        intra(s)
        chain_slot(2 * seqs + s)

        @pl.when(s == seqs // 2)
        def _():
            pass_r(unit_g)

        return carry

    lax.fori_loop(0, seqs, intra_later, 0)
    pass_y(unit_o)
    arrived(unit_g)
    project(unit_g, g_ref, 0, cols // half)
    arrived(unit_o)

    def ending(t, carry):
        done = target(3 * seqs - 1)

        def goal(t):
            return jnp.maximum(jnp.minimum(total - seqs + 2 * t + 4, total), done)

        before = jnp.where(t == 0, done, goal(t - 1))
        lax.fori_loop(before, goal(t), chain, 0)
        for g in range(groups):
            for b in range(2):
                t_copy(g * seqs + 2 * t + b).wait_recv()
        return finish(t, carry)

    lax.fori_loop(0, seqs // 2, ending, 0)

    for offset in range(1, n):
        e_copy(offset).wait_send()
    for j in range(own):
        holder_target, _ = place(j)

        @pl.when(me != holder_target)
        def _():
            i_copy(j).wait_send()

    for u in range(units):
        s_own(u).wait_send()
        for k in range(peers):
            y_copy(u, k).wait_send()
            s_copy(u, k, 0).wait_send()
            if axes[u] is not None:
                r_copy(u, k).wait_send()
                s_copy(u, k, 1).wait_send()
    for g in range(groups):
        d_copy(g).wait_send()

    def drain(k, carry):
        b_copy(k).wait_send()
        t_copy(k).wait_send()

        @pl.when(level < levels - 1)
        def _():
            c_copy(k).wait_send()

        return carry

    lax.fori_loop(0, total, drain, 0)


def body(
    n,
    ways,
    tokens,
    pre_gain,
    w_query,
    w_forget,
    w_value,
    w_gate,
    lower_bound,
    extra_decay,
    initial_state,
    norm_gain,
    w_out,
    post_gain,
):
    seqs, length, width = tokens.shape
    own, hk, hv = initial_state.shape
    items = own * n
    heads = items // seqs
    groups = heads // 2
    half = 2 * hk
    cols = heads * hk
    rows = seqs * length
    total = groups * seqs
    peers = max(ways // 2 - 1, 1)
    axes = ("x", "x") + ("z", "z") * (groups - 1) + ("z", "z", None)
    units = len(axes)
    dma = pltpu.SemaphoreType.DMA
    bf16, f32 = jnp.bfloat16, jnp.float32
    small = (
        pre_gain[None, :],
        lower_bound[None, :],
        norm_gain[None, :],
        post_gain[None, :],
    )
    shapes = [(width, half)] * (2 * groups) + [(width, cols)] * 2 + [(cols, width)]
    out = pl.pallas_call(
        functools.partial(layer_kernel, n, ways, heads, axes),
        out_shape=jax.ShapeDtypeStruct((rows, width), bf16),
        in_specs=[pl.BlockSpec(memory_space=pltpu.HBM)] * 12,
        out_specs=pl.BlockSpec(memory_space=pltpu.VMEM),
        scratch_shapes=[pltpu.VMEM(shape, bf16) for shape in shapes]
        + [
            pltpu.VMEM(tokens.shape, bf16),
            pltpu.VMEM((1, width), f32),
            pltpu.VMEM(extra_decay.shape, f32),
            pltpu.VMEM((1, cols), f32),
            pltpu.VMEM(initial_state.shape, f32),
            pltpu.VMEM((1, hv), f32),
            pltpu.VMEM((1, width), f32),
            pltpu.VMEM((rows, width), bf16),
            pltpu.VMEM((rows, cols), bf16),
            pltpu.VMEM((rows, cols), bf16),
            pltpu.VMEM((rows, cols), bf16),
            pltpu.VMEM((rows, cols), bf16),
            pltpu.VMEM((rows, cols), bf16),
            pltpu.VMEM((rows, cols), f32),
            pltpu.VMEM((seqs, cols), f32),
            pltpu.VMEM((seqs, cols), f32),
            pltpu.VMEM((rows, cols), f32),
            pltpu.VMEM((2 * length, cols), bf16),
            pltpu.VMEM((2 * length, width), f32),
            pltpu.VMEM((n, own, 128), f32),
            pltpu.VMEM((n, own, 128), f32),
            pltpu.VMEM((n, 128, own), f32),
            pltpu.VMEM((own, hv, hk), bf16),
            pltpu.VMEM((total, 2, hv, hk), bf16),
            pltpu.VMEM((total, hv, hk), bf16),
            pltpu.VMEM((total, 2, hv, hk), bf16),
            pltpu.VMEM((total, hv, hk), bf16),
            pltpu.VMEM((total, hv, hk), bf16),
            pltpu.VMEM((2, groups, seqs, hk), f32),
            pltpu.VMEM((groups, seqs, hk), f32),
            dma((units + 7,)),
            dma((units, peers)),
            dma((units, peers)),
            dma((units, peers)),
            dma((units, peers)),
            dma((units, 1 + 2 * peers)),
            dma((units, 1 + 2 * peers)),
            dma((n - 1,)),
            dma((n - 1,)),
            dma((own,)),
            dma((total,)),
            dma((total,)),
            dma((groups,)),
            dma((groups,)),
            dma((total,)),
            dma((total,)),
            dma((total,)),
            dma((total,)),
        ],
        compiler_params=pltpu.CompilerParams(
            collective_id=0, has_side_effects=True, vmem_limit_bytes=67043328 - rows * width * 2
        ),
        cost_estimate=pl.CostEstimate(
            flops=6 * 10**9, bytes_accessed=2 * 10**7, transcendentals=10**6
        ),
    )(
        tokens,
        small[0],
        w_forget,
        w_value,
        w_query,
        w_gate,
        w_out,
        extra_decay,
        small[1],
        initial_state,
        small[2],
        small[3],
    )
    return out.reshape(seqs, length, width)


def solution(mesh):
    in_specs = (
        P("dp", "sp", None),
        P(),
        P("dp", None),
        P("dp", None),
        P("dp", None),
        P("dp", None),
        P(),
        P(("dp", "sp"), None),
        P(("dp", "sp"), None, None),
        P(),
        P("dp", None),
        P(),
    )
    out_specs = P("dp", "sp", None)
    return jax.shard_map(
        functools.partial(body, mesh.shape["sp"], mesh.shape["dp"]),
        mesh=mesh,
        in_specs=in_specs,
        out_specs=out_specs,
        check_vma=False,
    )
```

time: 111 us -> 70.3 us (0.63)
  Pallas kernels: 98.3 us -> 67 us
  local copies, waits for them, and re-layouts: 8.89 us -> 3.16 us
  other arithmetic: 1.74 us -> 0 us
  matrix products: 1.35 us -> 0 us
    pallas_call x1, Pallas kernels: 98.3 us -> 67 us  [body(): pl.pallas_call(functools.partial(layer_kernel, n, ways, heads, axes), out...]
    unnamed x22 -> x1, local copies, waits for them, and re-layouts: 8.89 us -> 3.16 us
    convert_element_type x1 -> x0, other arithmetic: 1.73 us -> none  [body(): rms_scale(mixed, post_gain).astype(jnp.bfloat16)]
    dot_general x1 -> x0, matrix products: 1.35 us -> none  [body(): mixed = jnp.dot(gated, w_o, preferred_element_type=jnp.float32)]
where the time goes in v1:
time: 70.3 us; the launch traced here: 70.1 us
  Pallas kernels  67 us (95%)
  local copies, waits for them, and re-layouts  3.16 us (4%)
    pallas_call x1, Pallas kernels, body(): pl.pallas_call(functools.partial(layer_kernel, n, ways, heads, axes), out...  67 us
    unnamed x1, local copies, waits for them, and re-layouts  3.16 us

profile of v1, /device:TPU:26, one launch (start us, length us, event | category | flops | bytes accessed | tf_op | source)
XLA Modules:
  0.0 70.1 jit_solution(2678594673254936488)
XLA Ops:
  0.0 67.0 %shard_map.118 = bf16[512,2048]{1,0:T(8,128)(2,1)} custom-call(bf16[8,64,2048]{2,1,0:T(8,128)(2,1)} %tokens_hbm.1, f32[1,2048]{1,0:T(1,128)} %bitcast.6, bf16[512,512]{1,0:T(8,128)(2,1)} %wf_hbm.1, bf16[512,512]{1,0:T(8,128)(2,1)} %wv_hbm.1, bf16[512,512]{1,0:T(8,128)(2,1)} %wq_hbm.1, bf16[512,512]{1,0:T(8,128)(2,1)} %wg_hbm.1, bf16[128,2048]{1,0:T(8,128)(2,1)} %wo_hbm.1, ...), custom_call_target="tpu_custom_call" | custom-call | flops 6000000000 | bytes 20000000 | tf_op jit(solution)/shard_map/pallas_call | solution.py:624
  67.0 3.2 %copy.14 = bf16[8,64,2048]{2,1,0:T(8,128)(2,1)} copy(bf16[8,64,2048]{2,1,0:T(8,128)(2,1)} %bitcast.5) | data formatting | bytes 4194304

commit v2 on v1

v2 whole, which is shorter than its diff:
```python
import functools

import jax
import jax.numpy as jnp
from jax import lax
from jax.experimental import pallas as pl
from jax.experimental.pallas import tpu as pltpu
from jax.sharding import PartitionSpec as P

EPS = 1e-06
MESH = pl.DeviceIdType.MESH
NT = (((1,), (1,)), ((), ()))
TN = (((0,), (0,)), ((), ()))


def rms_scale(matrix, gain):
    widened = matrix.astype(jnp.float32)
    return widened * lax.rsqrt(jnp.mean(widened * widened, axis=-1, keepdims=True) + EPS) * gain


def layer_kernel(
    n,
    ways,
    heads,
    axes,
    tokens_hbm,
    pre_hbm,
    wf_hbm,
    wv_hbm,
    wq_hbm,
    wg_hbm,
    wo_hbm,
    extra_hbm,
    bound_hbm,
    init_hbm,
    gain_hbm,
    out_ref,
    *scratch,
):
    units = len(axes)
    groups = heads // 2
    wholes = scratch[:units]
    (
        tokens_ref,
        pre_ref,
        raw_ref,
        bound_ref,
        start_ref,
        gain_ref,
        normed,
        f_ref,
        v_ref,
        q_ref,
        g_ref,
        keys_ref,
        rel_ref,
        gap_ref,
        emid_ref,
        eend_ref,
        within_ref,
        gated_ref,
        esend,
        erecv,
        extra_ref,
        isend,
        st,
        fin,
        bb,
        bs,
        ob,
        dbuf,
        dsend,
        local_sem,
        y_send,
        y_recv,
        r_send,
        r_recv,
        s_send,
        s_recv,
        e_send,
        e_recv,
        i_send,
        b_send,
        b_recv,
        d_send,
        d_recv,
        c_send,
        c_recv,
        t_send,
        t_recv,
        up_sem,
        down_sem,
    ) = scratch[units:]
    me = lax.axis_index("sp")
    rank = lax.axis_index("dp")
    seqs, length, width = tokens_ref.shape
    own, hk, hv = start_ref.shape
    half = 2 * hk
    total = groups * seqs
    levels = n // 2
    side = lax.rem(me, 2)
    level = me // 2
    parity = lax.rem(level, 2)
    beside = me + 1 - 2 * side
    above = lax.rem(me + 2, n)
    below = lax.rem(me + n - 2, n)
    sibling = rank + 1 - 2 * lax.rem(rank, 2)
    peers = ways // 2 - 1
    not_top = level < levels - 1
    not_base = level > 0
    second_top = level == levels - 2
    unit_f = 4
    unit_q = unit_f + 2 * (groups - 1)
    unit_g = unit_q + groups
    unit_o = unit_g + groups

    def group_cols(base, g):
        return base.at[:, g * half : (g + 1) * half]

    def source(u):
        if u < 4:
            base = wf_hbm if u % 2 == 0 else wv_hbm
            head = side if u >= 2 else 1 - side
            return base.at[:, pl.ds(pl.multiple_of(head * hk, hk), hk)]
        if u < unit_q:
            return group_cols(wf_hbm if u % 2 == 0 else wv_hbm, (u - unit_f) // 2 + 1)
        if u < unit_g:
            return group_cols(wq_hbm, u - unit_q)
        if u < unit_o:
            return group_cols(wg_hbm, u - unit_g)
        part = width // 2
        return wo_hbm.at[:, (u - unit_o) * part : (u - unit_o + 1) * part]

    def full(u, shard):
        rows = wholes[u].shape[0] // ways
        return wholes[u].at[pl.ds(pl.multiple_of(shard * rows, rows), rows)]

    def part(u, shard, which):
        rows = wholes[u].shape[0] // ways
        start = shard * rows + which * (rows // 2)
        return wholes[u].at[pl.ds(pl.multiple_of(start, rows // 2), rows // 2)]

    def local_copy(u):
        return pltpu.make_async_copy(source(u), full(u, rank), local_sem.at[min(u, 2)])

    small = [
        pltpu.make_async_copy(src, dst, local_sem.at[3 + j])
        for j, (src, dst) in enumerate(
            (
                (tokens_hbm, tokens_ref),
                (pre_hbm, pre_ref),
                (extra_hbm, raw_ref),
                (init_hbm, start_ref),
                (bound_hbm, bound_ref),
                (gain_hbm, gain_ref),
            )
        )
    ]
    for u in (0, 1):
        local_copy(u).start()
    small[0].start()
    small[1].start()
    for u in range(2, units):
        local_copy(u).start()
    for copy in small[2:]:
        copy.start()

    barrier = pltpu.get_barrier_semaphore()

    def greet(device):
        pl.semaphore_signal(barrier, inc=1, device_id=device, device_id_type=MESH)

    greet({"sp": beside})
    for offset in range(1, ways):
        greet({"dp": lax.rem(rank + offset, ways)})

    @pl.when(not_top)
    def _():
        greet({"sp": above})

    @pl.when(not_base)
    def _():
        greet({"sp": below})

    pl.semaphore_wait(
        barrier, ways + not_top.astype(jnp.int32) + not_base.astype(jnp.int32)
    )

    def remote(src, dst, send, recv, device):
        return pltpu.make_async_remote_copy(
            src_ref=src,
            dst_ref=dst,
            send_sem=send,
            recv_sem=recv,
            device_id=device,
            device_id_type=MESH,
        )

    def settle(sem, rows, ref=None):
        ref = out_ref if ref is None else ref
        if rows:
            view = ref.at[0:rows]
            pltpu.make_async_copy(view, view, sem).wait()

    def bulk(us, halves=False):
        line = width * 4
        size = sum(wholes[u].shape[0] // ways * wholes[u].shape[1] * 2 for u in us)
        return size // (2 if halves else 1) // line

    z_units = [u for u in range(units) if axes[u] == "z"]

    def first_part(u, shard):
        return part(u, shard, parity) if axes[u] == "z" else full(u, shard)

    def y_copy(u, k):
        ref = first_part(u, rank)
        target = lax.rem(rank + 2 * (k + 1), ways)
        return remote(ref, ref, y_send.at[k], y_recv.at[u, k], {"dp": target})

    def origin(k):
        return lax.rem(rank + ways - 2 * (k + 1), ways)

    def m_copy(u, k):
        src, dst = full(u, origin(k)), full(u + 2, origin(k))
        return remote(src, dst, r_send.at[0, k], r_recv.at[u + 2, k], {"sp": beside})

    def z_copy(u, k, upward):
        ref = part(u, origin(k), parity)
        device = {"sp": above if upward else below}
        return remote(ref, ref, r_send.at[1 + upward, k], r_recv.at[u, k], device)

    def relay(u, k):
        if axes[u] == "y":
            m_copy(u, k).start()
        if axes[u] == "z":

            @pl.when(not_base)
            def _():
                z_copy(u, k, 0).start()

            @pl.when(second_top)
            def _():
                z_copy(u, k, 1).start()

    def s_own(u):
        ref = full(u, rank)
        return remote(ref, ref, s_send.at[0], s_recv.at[u], {"dp": sibling})

    def s_copy(u, k, second):
        ref = part(u, origin(k), 1 - parity) if second else first_part(u, origin(k))
        return remote(ref, ref, s_send.at[1 + k], s_recv.at[u], {"dp": sibling})

    def pass_y(u):
        for k in range(peers):
            y_copy(u, k).wait_recv()
            relay(u, k)
            s_copy(u, k, 0).start()

    def pass_r(u):
        for k in range(peers):
            if axes[u] == "m":
                m_copy(u - 2, k).wait_recv()
                s_copy(u, k, 0).start()
            else:
                z_copy(u, k, 0).wait_recv()
                s_copy(u, k, 1).start()

    def arrived(u):
        settle(s_recv.at[u], wholes[u].shape[0] // 2, wholes[u])

    def e_copy(offset):
        target = lax.rem(me + offset, n)
        return remote(
            esend.at[target],
            erecv.at[me],
            e_send,
            e_recv.at[offset - 1],
            {"sp": target},
        )

    near = jnp.where(side == 0, 1, n - 1)

    def place(j):
        it = me * own + j
        h = lax.rem(it, heads)
        return lax.rem(h, 2), (h // 2) * seqs + it // heads

    def i_copy(j):
        target, k = place(j)
        return remote(isend.at[j], st.at[k, 0], i_send.at[j], c_recv.at[k], {"sp": target})

    def b_copy(k):
        return remote(bs.at[k], bb.at[k, side], b_send, b_recv.at[k], {"sp": beside})

    def d_copy(g):
        return remote(dsend.at[g], dbuf.at[side, g], d_send, d_recv.at[g], {"sp": beside})

    def c_copy(k):
        return remote(ob.at[k], st.at[k, 0], c_send, c_recv.at[k], {"sp": above})

    def t_copy(k):
        return remote(st.at[k, 1 - side], fin.at[k], t_send, t_recv.at[k], {"sp": beside})

    for u in range(units):
        if u < 2:
            local_copy(u).wait()
        if u == 2:
            settle(local_sem.at[2], bulk(range(2, units)))
        if axes[u] != "m":
            for k in range(peers):
                y_copy(u, k).start()
        s_own(u).start()

    def tell(sem, device):
        pl.semaphore_signal(sem, inc=1, device_id={"sp": device}, device_id_type=MESH)

    @pl.when(jnp.logical_not(not_base))
    def _():
        tell(up_sem, above)

    @pl.when(jnp.logical_not(not_top))
    def _():
        tell(down_sem, below)

    @pl.when(not_base)
    def _():
        pl.semaphore_wait(up_sem, 1)

        @pl.when(not_top)
        def _():
            tell(up_sem, above)
            pl.semaphore_wait(down_sem, 1)
            tell(down_sem, below)

    for copy in small:
        copy.wait()

    def norm_rows(s, carry):
        rows = pl.ds(pl.multiple_of(s * length, length), length)
        normed[rows, :] = rms_scale(tokens_ref[s], pre_ref[...]).astype(jnp.bfloat16)
        return carry

    def send_extras():
        for offset in range(1, n):

            @pl.when(offset != near)
            def _():
                e_copy(offset).start()

    def send_states():
        for j in range(own):
            target, k = place(j)

            @pl.when(me != target)
            def _():
                i_copy(j).start()

            @pl.when(me == target)
            def _():
                st[k, 0] = isend[j]

    pad = esend.shape[2]
    for p in range(n):
        piece = raw_ref[:, p * length : (p + 1) * length]
        esend[p] = jnp.concatenate(
            [piece, jnp.zeros((own, pad - length), jnp.float32)], axis=1
        )
    e_copy(near).start()

    @pl.when(not_base)
    def _():
        send_extras()

    for j in range(own):
        isend[j] = start_ref[j].T.astype(jnp.bfloat16)
    for h in range(heads):
        gap_ref[h] = 1.0 - bound_ref[:, h * hk : (h + 1) * hk]
    erecv[me] = esend[me]

    lax.fori_loop(0, seqs, norm_rows, 0)

    @pl.when(level < 2)
    def _():
        send_states()

    pass_y(0)

    @pl.when(jnp.logical_not(not_base))
    def _():
        pl.semaphore_wait(down_sem, 1)
        send_extras()

    row = lax.broadcasted_iota(jnp.int32, (length, length), 0)
    col = lax.broadcasted_iota(jnp.int32, (length, length), 1)
    causal = row >= col
    ones = causal.astype(jnp.bfloat16)
    ones = jnp.concatenate([ones, ones], axis=1)
    middle = length // 2

    def seq_rows(s):
        return pl.ds(pl.multiple_of(s * length, length), length)

    def head_of(g, role):
        return 2 * g + (side if role == 0 else 1 - side)

    def head_lanes(g, role):
        return pl.ds(pl.multiple_of(head_of(g, role) * hk, hk), hk)

    def project(u, dest, lanes):
        dest[:, lanes] = jnp.dot(
            normed[...], wholes[u][...], preferred_element_type=jnp.float32
        ).astype(jnp.bfloat16)

    def group_lanes(g):
        return slice(g * half, (g + 1) * half)

    def extras(s):
        for j in range(heads // own):
            p = s * (heads // own) + j
            offset = lax.rem(me - p + n, n)

            @pl.when(offset > 0)
            def _():
                e_copy(offset).wait_recv()

            extra_ref[p] = erecv[p].T

    def decays(g, role, s):
        rows = seq_rows(s)
        lanes = head_lanes(g, role)
        head = head_of(g, role)
        keys = gap_ref[head] * jax.nn.sigmoid(-f_ref[rows, lanes].astype(jnp.float32))
        columns = [
            extra_ref[s * (heads // own) + h // own][:length, h % own : h % own + 1]
            for h in (2 * g, 2 * g + 1)
        ]
        spread = jnp.where(side == role, columns[0], columns[1])
        decay = jnp.log(1.0 - keys) + spread
        high = decay.astype(jnp.bfloat16)
        low = (decay - high.astype(jnp.float32)).astype(jnp.bfloat16)
        cum = jnp.dot(
            ones, jnp.concatenate([high, low], axis=0), preferred_element_type=jnp.float32
        )
        mid = cum[middle : middle + 1, :]
        end = cum[length - 1 : length, :]
        rel = cum - mid
        keys_ref[rows, lanes] = (keys * jnp.exp(-rel)).astype(jnp.bfloat16)
        rel_ref[rows, lanes] = rel
        emid_ref[head, pl.ds(s, 1)] = jnp.exp(mid)
        eend_ref[head, pl.ds(s, 1)] = jnp.exp(end - mid)
        if role == 0:
            dbuf[side, g, pl.ds(s, 1)] = jnp.exp(end)
        else:
            dsend[g, pl.ds(s, 1)] = jnp.exp(end)

    def added(g, role, s):
        rows = seq_rows(s)
        lanes = head_lanes(g, role)
        state = lax.dot_general(
            v_ref[rows, lanes], keys_ref[rows, lanes], TN, preferred_element_type=jnp.float32
        )
        return (state * eend_ref[head_of(g, role), pl.ds(s, 1)]).astype(jnp.bfloat16)

    def local_sent(g, s):
        k = g * seqs + s
        bs[k] = added(g, 1, s)
        b_copy(k).start()

    def local_kept(g, s):
        bb[g * seqs + s, side] = added(g, 0, s)

    def chain(k, carry):
        g = k // seqs
        s = lax.rem(k, seqs)
        holder = (s * heads + 2 * g + side) // own
        b_copy(k).wait_recv()

        @pl.when(jnp.logical_or(not_base, holder != me))
        def _():
            c_copy(k).wait_recv()

        first = dbuf[0, g, pl.ds(s, 1)]
        between = st[k, 0].astype(jnp.float32) * first + bb[k, 0].astype(jnp.float32)
        st[k, 1] = between.astype(jnp.bfloat16)
        t_copy(k).start()

        @pl.when(not_top)
        def _():
            second = dbuf[1, g, pl.ds(s, 1)]
            ob[k] = (between * second + bb[k, 1].astype(jnp.float32)).astype(jnp.bfloat16)
            c_copy(k).start()

        return carry

    def reached(g, time):
        begin = 182 + 93 * g + jnp.where(not_base, 14 + 18 * level, 0)
        return g * seqs + jnp.clip(time - begin + 7, 0, 7 * seqs) // 7

    def advance(before, now):
        for g in range(groups):
            lax.fori_loop(reached(g, before), reached(g, now), chain, 0)

    def intra(s):
        rows = seq_rows(s)
        for h in range(heads):
            lanes = slice(h * hk, (h + 1) * hk)
            q_pre = q_ref[rows, lanes].astype(jnp.float32)
            q_mid = q_pre * jax.nn.sigmoid(q_pre) * jnp.exp(rel_ref[rows, lanes])
            q_ref[rows, lanes] = (q_mid * emid_ref[h, pl.ds(s, 1)]).astype(jnp.bfloat16)
            scores = lax.dot_general(
                q_mid.astype(jnp.bfloat16),
                keys_ref[rows, lanes],
                NT,
                preferred_element_type=jnp.float32,
            )
            scores = jnp.where(causal, scores, 0.0).astype(jnp.bfloat16)
            within_ref[rows, lanes] = jnp.dot(
                scores, v_ref[rows, lanes], preferred_element_type=jnp.float32
            )

    def finish(t, carry):
        for b in range(2):
            s = 2 * t + b
            rows = seq_rows(s)
            for g in range(groups):
                k = g * seqs + s
                for role in range(2):
                    lanes = head_lanes(g, role)
                    state = st[k, side] if role == 0 else fin[k]
                    outs = within_ref[rows, lanes] + lax.dot_general(
                        q_ref[rows, lanes], state, NT, preferred_element_type=jnp.float32
                    )
                    scaled = rms_scale(outs, gain_ref[...]).astype(jnp.bfloat16)
                    g_pre = g_ref[rows, lanes].astype(jnp.float32)
                    gated_ref[b * length : (b + 1) * length, lanes] = (
                        scaled.astype(jnp.float32) * (g_pre * jax.nn.sigmoid(g_pre))
                    ).astype(jnp.bfloat16)
        tile = 512
        squares = jnp.zeros((2 * length, 1), jnp.float32)
        rows = pl.ds(pl.multiple_of(t * 2 * length, 2 * length), 2 * length)
        tiles = [
            (unit_o + p, slice(j * tile, (j + 1) * tile), p * (width // 2) + j * tile)
            for p in range(2)
            for j in range(width // 2 // tile)
        ]
        for u, lanes, at in tiles:
            mixed = jnp.dot(
                gated_ref[...], wholes[u][:, lanes], preferred_element_type=jnp.float32
            )
            squares = squares + jnp.sum(mixed * mixed, axis=-1, keepdims=True)
            out_ref[rows, at : at + tile] = mixed
        scale = lax.rsqrt(squares * (1.0 / width) + EPS)
        for u, lanes, at in tiles:
            out_ref[rows, at : at + tile] = out_ref[rows, at : at + tile] * scale
        return carry

    def loop(step, hooks=(), count=seqs):
        def run(s, carry):
            step(s)
            for at, act in hooks:

                @pl.when(s == at)
                def _():
                    act()

            return carry

        lax.fori_loop(0, count, run, 0)

    def paired(step):
        def run(t):
            step(2 * t)
            step(2 * t + 1)

        return run

    twos = seqs // 2
    arrived(0)
    project(0, f_ref, head_lanes(0, 1))
    pass_y(1)

    def first_decays(t):
        for s in (2 * t, 2 * t + 1):
            extras(s)
        for s in (2 * t, 2 * t + 1):
            decays(0, 1, s)

    loop(first_decays, count=twos)
    d_copy(0).start()
    arrived(1)
    project(1, v_ref, head_lanes(0, 1))
    pass_y(4)

    @pl.when(level >= 2)
    def _():
        send_states()

    loop(paired(lambda s: local_sent(0, s)), count=twos)
    pass_r(2)
    arrived(2)
    project(2, f_ref, head_lanes(0, 0))
    loop(paired(lambda s: decays(0, 0, s)), ((twos - 1, lambda: pass_r(3)),), count=twos)
    pass_y(5)
    arrived(3)
    project(3, v_ref, head_lanes(0, 0))
    d_copy(0).wait_recv()
    loop(paired(lambda s: local_kept(0, s)), count=twos)
    pass_r(4)
    pass_y(6)
    arrived(4)
    project(4, f_ref, group_lanes(1))
    advance(0, 205)

    def later_other(t):
        decays(1, 1, 2 * t)
        decays(1, 1, 2 * t + 1)
        advance(205 + 3 * t, 208 + 3 * t)

    def later_mine(t):
        decays(1, 0, 2 * t)
        decays(1, 0, 2 * t + 1)
        advance(239 + 3 * t, 242 + 3 * t)

    def later_sent(t):
        local_sent(1, 2 * t)
        local_sent(1, 2 * t + 1)
        advance(227 + 3 * t, 230 + 3 * t)

    def later_kept(t):
        local_kept(1, 2 * t)
        local_kept(1, 2 * t + 1)
        advance(251 + 3 * t, 254 + 3 * t)

    loop(later_other, count=twos)
    d_copy(1).start()
    pass_r(5)
    pass_y(7)
    arrived(5)
    project(5, v_ref, group_lanes(1))
    advance(205 + 3 * twos, 227)
    pass_y(8)
    loop(later_sent, count=twos)
    loop(later_mine, count=twos)
    pass_y(9)
    pass_r(6)
    loop(later_kept, count=twos)
    pass_y(10)
    d_copy(1).wait_recv()
    time = 251 + 3 * twos
    pass_r(7)
    arrived(6)
    project(6, q_ref, group_lanes(0))
    advance(time, 275)
    arrived(7)
    project(7, q_ref, group_lanes(1))
    advance(275, 293)
    pass_r(8)
    pass_y(11)

    def intra_slot(s):
        intra(s)
        advance(293 + 6 * s, 299 + 6 * s)

    loop(
        intra_slot,
        (
            (seqs // 2, lambda: pass_r(9)),
            (seqs - 2, lambda: pass_r(10)),
        ),
    )
    time = 293 + 6 * seqs
    arrived(8)
    project(8, g_ref, group_lanes(0))
    advance(time, 356)
    arrived(9)
    project(9, g_ref, group_lanes(1))
    advance(356, 368)
    lax.fori_loop(reached(0, 368), seqs, chain, 0)
    done = jnp.where(not_top, total, reached(1, 368))
    lax.fori_loop(reached(1, 368), done, chain, 0)
    pass_r(11)

    settle(e_send, n - 1, esend)
    for j in range(own):
        holder_target, _ = place(j)

        @pl.when(me != holder_target)
        def _():
            i_copy(j).wait_send()

    settle(d_send, groups, dsend)
    settle(b_send, total, bs)
    settle(s_send.at[0], bulk(range(units)))
    for k in range(peers):
        settle(y_send.at[k], bulk((0, 1)) + bulk(z_units, True))
        settle(r_send.at[0, k], bulk((0, 1)))
        settle(s_send.at[1 + k], bulk(range(units)))

        @pl.when(not_base)
        def _():
            settle(r_send.at[1, k], bulk(z_units, True))

        @pl.when(second_top)
        def _():
            settle(r_send.at[2, k], bulk(z_units, True))

    arrived(10)
    arrived(11)

    def ending(t, carry):
        def goal(t):
            return jnp.maximum(seqs + jnp.minimum(2 * t + 4, seqs), done)

        lax.fori_loop(jnp.where(t == 0, done, goal(t - 1)), goal(t), chain, 0)
        for g in range(groups):
            for b in range(2):
                t_copy(g * seqs + 2 * t + b).wait_recv()
        return finish(t, carry)

    lax.fori_loop(0, seqs // 2, ending, 0)

    settle(t_send, total, fin)

    @pl.when(not_top)
    def _():
        settle(c_send, total, ob)


def body(
    n,
    ways,
    tokens,
    pre_gain,
    w_query,
    w_forget,
    w_value,
    w_gate,
    lower_bound,
    extra_decay,
    initial_state,
    norm_gain,
    w_out,
    post_gain,
):
    seqs, length, width = tokens.shape
    own, hk, hv = initial_state.shape
    items = own * n
    heads = items // seqs
    groups = heads // 2
    half = 2 * hk
    cols = heads * hk
    rows = seqs * length
    total = groups * seqs
    peers = max(ways // 2 - 1, 1)
    axes = ("y", "y", "m", "m") + ("z",) * (2 * (groups - 1) + 2 * groups + 2)
    units = len(axes)
    dma = pltpu.SemaphoreType.DMA
    bf16, f32 = jnp.bfloat16, jnp.float32
    shapes = [(width, hk)] * 4 + [(width, half)] * (4 * groups - 2) + [(cols, width // 2)] * 2
    out = pl.pallas_call(
        functools.partial(layer_kernel, n, ways, heads, axes),
        out_shape=pltpu.VMEM((rows, width), f32),
        in_specs=[pl.BlockSpec(memory_space=pltpu.HBM)] * 11,
        out_specs=pl.BlockSpec(memory_space=pltpu.VMEM),
        scratch_shapes=[pltpu.VMEM(shape, bf16) for shape in shapes]
        + [
            pltpu.VMEM(tokens.shape, bf16),
            pltpu.VMEM((1, width), f32),
            pltpu.VMEM(extra_decay.shape, f32),
            pltpu.VMEM((1, cols), f32),
            pltpu.VMEM(initial_state.shape, f32),
            pltpu.VMEM((1, hv), f32),
            pltpu.VMEM((rows, width), bf16),
            pltpu.VMEM((rows, cols), bf16),
            pltpu.VMEM((rows, cols), bf16),
            pltpu.VMEM((rows, cols), bf16),
            pltpu.VMEM((rows, cols), bf16),
            pltpu.VMEM((rows, cols), bf16),
            pltpu.VMEM((rows, cols), f32),
            pltpu.VMEM((heads, 1, hk), f32),
            pltpu.VMEM((heads, seqs, hk), f32),
            pltpu.VMEM((heads, seqs, hk), f32),
            pltpu.VMEM((rows, cols), f32),
            pltpu.VMEM((2 * length, cols), bf16),
            pltpu.VMEM((n, own, 128), f32),
            pltpu.VMEM((n, own, 128), f32),
            pltpu.VMEM((n, 128, own), f32),
            pltpu.VMEM((own, hv, hk), bf16),
            pltpu.VMEM((total, 2, hv, hk), bf16),
            pltpu.VMEM((total, hv, hk), bf16),
            pltpu.VMEM((total, 2, hv, hk), bf16),
            pltpu.VMEM((total, hv, hk), bf16),
            pltpu.VMEM((total, hv, hk), bf16),
            pltpu.VMEM((2, groups, seqs, hk), f32),
            pltpu.VMEM((groups, seqs, hk), f32),
            dma((9,)),
            dma((peers,)),
            dma((units, peers)),
            dma((3, peers)),
            dma((units, peers)),
            dma((1 + peers,)),
            dma((units,)),
            dma(()),
            dma((n - 1,)),
            dma((own,)),
            dma(()),
            dma((total,)),
            dma(()),
            dma((groups,)),
            dma(()),
            dma((total,)),
            dma(()),
            dma((total,)),
            pltpu.SemaphoreType.REGULAR,
            pltpu.SemaphoreType.REGULAR,
        ],
        compiler_params=pltpu.CompilerParams(
            collective_id=0,
            has_side_effects=True,
            vmem_limit_bytes=67043328 - rows * width * 4 - 2**18,
        ),
        cost_estimate=pl.CostEstimate(
            flops=6 * 10**9, bytes_accessed=2 * 10**7, transcendentals=10**6
        ),
    )(
        tokens,
        pre_gain[None, :],
        w_forget,
        w_value,
        w_query,
        w_gate,
        w_out,
        extra_decay,
        lower_bound[None, :],
        initial_state,
        norm_gain[None, :],
    )
    return (out * post_gain).astype(bf16).reshape(seqs, length, width)


def solution(mesh):
    in_specs = (
        P("dp", "sp", None),
        P(),
        P("dp", None),
        P("dp", None),
        P("dp", None),
        P("dp", None),
        P(),
        P(("dp", "sp"), None),
        P(("dp", "sp"), None, None),
        P(),
        P("dp", None),
        P(),
    )
    out_specs = P("dp", "sp", None)
    return jax.shard_map(
        functools.partial(body, mesh.shape["sp"], mesh.shape["dp"]),
        mesh=mesh,
        in_specs=in_specs,
        out_specs=out_specs,
        check_vma=False,
    )
```

time: 70.3 us -> 62.7 us (0.89)
  Pallas kernels: 67 us -> 60.7 us
  local copies, waits for them, and re-layouts: 3.16 us -> 0.01 us
  other arithmetic: 0 us -> 1.82 us
    pallas_call x1, Pallas kernels: 67 us -> 60.7 us  [body(): pl.pallas_call(functools.partial(layer_kernel, n, ways, heads, axes), out...]
    unnamed x1 -> x2, local copies, waits for them, and re-layouts: 3.16 us -> 0.01 us
    convert_element_type x0 -> x1, other arithmetic: none -> 1.82 us  [body(): return (out * post_gain).astype(bf16).reshape(seqs, length, width)]
where the time goes in v2:
time: 62.7 us; the launch traced here: 62.5 us
  Pallas kernels  60.7 us (97%)
  other arithmetic  1.82 us (3%)
    pallas_call x1, Pallas kernels, body(): pl.pallas_call(functools.partial(layer_kernel, n, ways, heads, axes), out...  60.7 us
    convert_element_type x1, other arithmetic, body(): return (out * post_gain).astype(bf16).reshape(seqs, length, width)  1.82 us

profile of v2, /device:TPU:26, one launch (start us, length us, event | category | flops | bytes accessed | tf_op | source)
XLA Modules:
  0.0 62.5 jit_solution(2587063779160714898)
XLA Ops:
  0.0 0.0 copy-start
  0.0 60.7 %shard_map.118 = f32[512,2048]{1,0:T(8,128)S(1)} custom-call(bf16[8,64,2048]{2,1,0:T(8,128)(2,1)} %tokens_hbm.1, f32[1,2048]{1,0:T(1,128)} %bitcast.4, bf16[512,512]{1,0:T(8,128)(2,1)} %wf_hbm.1, bf16[512,512]{1,0:T(8,128)(2,1)} %wv_hbm.1, bf16[512,512]{1,0:T(8,128)(2,1)} %wq_hbm.1, bf16[512,512]{1,0:T(8,128)(2,1)} %wg_hbm.1, bf16[128,2048]{1,0:T(8,128)(2,1)} %wo_hbm.1, ...), custom_call_target="tpu_custom_call" | custom-call | flops 6000000000 | bytes 20000000 | tf_op jit(solution)/shard_map/pallas_call | solution.py:760
  60.7 0.0 copy-done
  60.7 1.8 %multiply_convert_fusion = bf16[512,2048]{1,0:T(8,128)(2,1)} fusion(f32[512,2048]{1,0:T(8,128)S(1)} %shard_map.118, f32[2048]{0:T(1024)S(1)} %copy-done), kind=kLoop, calls=%fused_computation | loop fusion | flops 2097152 | bytes 6299648 | tf_op jit(solution)/shard_map/convert_element_type | solution.py:838
Async XLA Ops:
  0.0 60.7 %copy-start = (f32[2048]{0:T(1024)S(1)}, f32[2048]{0:T(1024)}, u32[]{:S(2)}) copy-start(f32[2048]{0:T(1024)} %param.23) | copy-start | bytes 24580

commit v3 on v2

--- a/solution.py
+++ b/solution.py
@@ -217,6 +217,11 @@
         target = lax.rem(rank + 2 * (k + 1), ways)
         return remote(ref, ref, y_send.at[k], y_recv.at[u, k], {"dp": target})
 
+    def y_rest(u, k):
+        ref = part(u, rank, 1 - parity)
+        target = lax.rem(rank + 2 * (k + 1), ways)
+        return remote(ref, ref, r_send.at[2, k], r_recv.at[u, k], {"dp": target})
+
     def origin(k):
         return lax.rem(rank + ways - 2 * (k + 1), ways)
 
@@ -238,9 +243,11 @@
             def _():
                 z_copy(u, k, 0).start()
 
-            @pl.when(second_top)
-            def _():
-                z_copy(u, k, 1).start()
+            if u < unit_g:
+
+                @pl.when(second_top)
+                def _():
+                    z_copy(u, k, 1).start()
 
     def s_own(u):
         ref = full(u, rank)
@@ -311,6 +318,12 @@
                 y_copy(u, k).start()
         s_own(u).start()
 
+    @pl.when(jnp.logical_not(not_top))
+    def _():
+        for u in range(unit_g, units):
+            for k in range(peers):
+                y_rest(u, k).start()
+
     def tell(sem, device):
         pl.semaphore_signal(sem, inc=1, device_id={"sp": device}, device_id_type=MESH)
 
@@ -321,16 +334,6 @@
     @pl.when(jnp.logical_not(not_top))
     def _():
         tell(down_sem, below)
-
-    @pl.when(not_base)
-    def _():
-        pl.semaphore_wait(up_sem, 1)
-
-        @pl.when(not_top)
-        def _():
-            tell(up_sem, above)
-            pl.semaphore_wait(down_sem, 1)
-            tell(down_sem, below)
 
     for copy in small:
         copy.wait()
@@ -340,10 +343,12 @@
         normed[rows, :] = rms_scale(tokens_ref[s], pre_ref[...]).astype(jnp.bfloat16)
         return carry
 
-    def send_extras():
+    def send_extras(upward):
         for offset in range(1, n):
-
-            @pl.when(offset != near)
+            there = lax.rem(me + offset, n) // 2
+            far = there > level if upward else there < level
+
+            @pl.when(far)
             def _():
                 e_copy(offset).start()
 
@@ -365,30 +370,38 @@
         esend[p] = jnp.concatenate(
             [piece, jnp.zeros((own, pad - length), jnp.float32)], axis=1
         )
+    for j in range(own):
+        isend[j] = start_ref[j].T.astype(jnp.bfloat16)
     e_copy(near).start()
 
     @pl.when(not_base)
     def _():
-        send_extras()
-
-    for j in range(own):
-        isend[j] = start_ref[j].T.astype(jnp.bfloat16)
+        pl.semaphore_wait(up_sem, 1)
+
+        @pl.when(not_top)
+        def _():
+            tell(up_sem, above)
+
+        send_extras(False)
+
+    send_states()
     for h in range(heads):
         gap_ref[h] = 1.0 - bound_ref[:, h * hk : (h + 1) * hk]
     erecv[me] = esend[me]
-
     lax.fori_loop(0, seqs, norm_rows, 0)
 
-    @pl.when(level < 2)
+    @pl.when(jnp.logical_and(not_base, not_top))
     def _():
-        send_states()
+        pl.semaphore_wait(down_sem, 1)
+        tell(down_sem, below)
+        send_extras(True)
 
     pass_y(0)
 
     @pl.when(jnp.logical_not(not_base))
     def _():
         pl.semaphore_wait(down_sem, 1)
-        send_extras()
+        send_extras(True)
 
     row = lax.broadcasted_iota(jnp.int32, (length, length), 0)
     col = lax.broadcasted_iota(jnp.int32, (length, length), 1)
@@ -493,7 +506,7 @@
         return carry
 
     def reached(g, time):
-        begin = 182 + 93 * g + jnp.where(not_base, 14 + 18 * level, 0)
+        begin = 182 + 81 * g + jnp.where(not_base, 10 + 22 * level, 0)
         return g * seqs + jnp.clip(time - begin + 7, 0, 7 * seqs) // 7
 
     def advance(before, now):
@@ -590,11 +603,6 @@
     arrived(1)
     project(1, v_ref, head_lanes(0, 1))
     pass_y(4)
-
-    @pl.when(level >= 2)
-    def _():
-        send_states()
-
     loop(paired(lambda s: local_sent(0, s)), count=twos)
     pass_r(2)
     arrived(2)
@@ -605,11 +613,12 @@
     project(3, v_ref, head_lanes(0, 0))
     d_copy(0).wait_recv()
     loop(paired(lambda s: local_kept(0, s)), count=twos)
+    advance(0, 197)
     pass_r(4)
     pass_y(6)
     arrived(4)
     project(4, f_ref, group_lanes(1))
-    advance(0, 205)
+    advance(197, 205)
 
     def later_other(t):
         decays(1, 1, 2 * t)
@@ -635,26 +644,27 @@
     d_copy(1).start()
     pass_r(5)
     pass_y(7)
+    advance(205 + 3 * twos, 224)
     arrived(5)
     project(5, v_ref, group_lanes(1))
-    advance(205 + 3 * twos, 227)
+    advance(224, 227)
     pass_y(8)
     loop(later_sent, count=twos)
     loop(later_mine, count=twos)
     pass_y(9)
     pass_r(6)
+    d_copy(1).wait_recv()
     loop(later_kept, count=twos)
     pass_y(10)
-    d_copy(1).wait_recv()
     time = 251 + 3 * twos
+    advance(time, time + 1)
     pass_r(7)
     arrived(6)
     project(6, q_ref, group_lanes(0))
-    advance(time, 275)
+    advance(time + 1, 275)
     arrived(7)
     project(7, q_ref, group_lanes(1))
     advance(275, 293)
-    pass_r(8)
     pass_y(11)
 
     def intra_slot(s):
@@ -664,8 +674,8 @@
     loop(
         intra_slot,
         (
-            (seqs // 2, lambda: pass_r(9)),
-            (seqs - 2, lambda: pass_r(10)),
+            (seqs // 2, lambda: pass_r(8)),
+            (seqs - 1, lambda: pass_r(9)),
         ),
     )
     time = 293 + 6 * seqs
@@ -678,6 +688,7 @@
     lax.fori_loop(reached(0, 368), seqs, chain, 0)
     done = jnp.where(not_top, total, reached(1, 368))
     lax.fori_loop(reached(1, 368), done, chain, 0)
+    pass_r(10)
     pass_r(11)
 
     settle(e_send, n - 1, esend)
@@ -702,7 +713,11 @@
 
         @pl.when(second_top)
         def _():
-            settle(r_send.at[2, k], bulk(z_units, True))
+            settle(r_send.at[2, k], bulk(range(unit_f, unit_g), True))
+
+        @pl.when(jnp.logical_not(not_top))
+        def _():
+            settle(r_send.at[2, k], bulk(range(unit_g, units), True))
 
     arrived(10)
     arrived(11)

time: 62.7 us -> 53.4 us (0.85)
  Pallas kernels: 60.7 us -> 51 us
    pallas_call x1, Pallas kernels: 60.7 us -> 51 us  [body(): pl.pallas_call(functools.partial(layer_kernel, n, ways, heads, axes), out...]
where the time goes in v3:
time: 53.4 us; the launch traced here: 52.8 us
  Pallas kernels  51 us (96%)
  other arithmetic  1.82 us (3%)
    pallas_call x1, Pallas kernels, body(): pl.pallas_call(functools.partial(layer_kernel, n, ways, heads, axes), out...  51 us
    convert_element_type x1, other arithmetic, body(): return (out * post_gain).astype(bf16).reshape(seqs, length, width)  1.82 us

profile of v3, /device:TPU:26, one launch (start us, length us, event | category | flops | bytes accessed | tf_op | source)
XLA Modules:
  0.0 52.8 jit_solution(17386545609896113193)
XLA Ops:
  0.0 0.0 copy-start
  0.0 51.0 %shard_map.118 = f32[512,2048]{1,0:T(8,128)S(1)} custom-call(bf16[8,64,2048]{2,1,0:T(8,128)(2,1)} %tokens_hbm.1, f32[1,2048]{1,0:T(1,128)} %bitcast.4, bf16[512,512]{1,0:T(8,128)(2,1)} %wf_hbm.1, bf16[512,512]{1,0:T(8,128)(2,1)} %wv_hbm.1, bf16[512,512]{1,0:T(8,128)(2,1)} %wq_hbm.1, bf16[512,512]{1,0:T(8,128)(2,1)} %wg_hbm.1, bf16[128,2048]{1,0:T(8,128)(2,1)} %wo_hbm.1, ...), custom_call_target="tpu_custom_call" | custom-call | flops 6000000000 | bytes 20000000 | tf_op jit(solution)/shard_map/pallas_call | solution.py:775
  51.0 0.0 copy-done
  51.0 1.8 %multiply_convert_fusion = bf16[512,2048]{1,0:T(8,128)(2,1)} fusion(f32[512,2048]{1,0:T(8,128)S(1)} %shard_map.118, f32[2048]{0:T(1024)S(1)} %copy-done), kind=kLoop, calls=%fused_computation | loop fusion | flops 2097152 | bytes 6299648 | tf_op jit(solution)/shard_map/convert_element_type | solution.py:853
Async XLA Ops:
  0.0 51.0 %copy-start = (f32[2048]{0:T(1024)S(1)}, f32[2048]{0:T(1024)}, u32[]{:S(2)}) copy-start(f32[2048]{0:T(1024)} %param.23) | copy-start | bytes 24580

commit v4 on v3

--- a/solution.py
+++ b/solution.py
@@ -34,6 +34,7 @@
     bound_hbm,
     init_hbm,
     gain_hbm,
+    post_hbm,
     out_ref,
     *scratch,
 ):
@@ -47,6 +48,8 @@
         bound_ref,
         start_ref,
         gain_ref,
+        post_ref,
+        mixed_ref,
         normed,
         f_ref,
         v_ref,
@@ -141,10 +144,10 @@
         return wholes[u].at[pl.ds(pl.multiple_of(start, rows // 2), rows // 2)]
 
     def local_copy(u):
-        return pltpu.make_async_copy(source(u), full(u, rank), local_sem.at[min(u, 2)])
+        return pltpu.make_async_copy(source(u), full(u, rank), local_sem.at[3 if u >= unit_g else min(u, 2)])
 
     small = [
-        pltpu.make_async_copy(src, dst, local_sem.at[3 + j])
+        pltpu.make_async_copy(src, dst, local_sem.at[4 + j])
         for j, (src, dst) in enumerate(
             (
                 (tokens_hbm, tokens_ref),
@@ -153,6 +156,7 @@
                 (init_hbm, start_ref),
                 (bound_hbm, bound_ref),
                 (gain_hbm, gain_ref),
+                (post_hbm, post_ref),
             )
         )
     ]
@@ -203,7 +207,7 @@
             pltpu.make_async_copy(view, view, sem).wait()
 
     def bulk(us, halves=False):
-        line = width * 4
+        line = width * 2
         size = sum(wholes[u].shape[0] // ways * wholes[u].shape[1] * 2 for u in us)
         return size // (2 if halves else 1) // line
 
@@ -251,11 +255,11 @@
 
     def s_own(u):
         ref = full(u, rank)
-        return remote(ref, ref, s_send.at[0], s_recv.at[u], {"dp": sibling})
+        return remote(ref, ref, s_send.at[u // unit_g, 0], s_recv.at[u], {"dp": sibling})
 
     def s_copy(u, k, second):
         ref = part(u, origin(k), 1 - parity) if second else first_part(u, origin(k))
-        return remote(ref, ref, s_send.at[1 + k], s_recv.at[u], {"dp": sibling})
+        return remote(ref, ref, s_send.at[u // unit_g, 1 + k], s_recv.at[u], {"dp": sibling})
 
     def pass_y(u):
         for k in range(peers):
@@ -312,7 +316,9 @@
         if u < 2:
             local_copy(u).wait()
         if u == 2:
-            settle(local_sem.at[2], bulk(range(2, units)))
+            settle(local_sem.at[2], bulk(range(2, unit_g)))
+        if u == unit_g:
+            settle(local_sem.at[3], bulk(range(unit_g, units)))
         if axes[u] != "m":
             for k in range(peers):
                 y_copy(u, k).start()
@@ -506,7 +512,8 @@
         return carry
 
     def reached(g, time):
-        begin = 182 + 81 * g + jnp.where(not_base, 10 + 22 * level, 0)
+        first, lag, hop = ((182, 10, 22), (258, 17, 20))[min(g, 1)]
+        begin = first + jnp.where(not_base, lag + hop * level, 0)
         return g * seqs + jnp.clip(time - begin + 7, 0, 7 * seqs) // 7
 
     def advance(before, now):
@@ -561,10 +568,12 @@
                 gated_ref[...], wholes[u][:, lanes], preferred_element_type=jnp.float32
             )
             squares = squares + jnp.sum(mixed * mixed, axis=-1, keepdims=True)
-            out_ref[rows, at : at + tile] = mixed
+            mixed_ref[:, at : at + tile] = mixed
         scale = lax.rsqrt(squares * (1.0 / width) + EPS)
         for u, lanes, at in tiles:
-            out_ref[rows, at : at + tile] = out_ref[rows, at : at + tile] * scale
+            out_ref[rows, at : at + tile] = (
+                mixed_ref[:, at : at + tile] * scale * post_ref[:, at : at + tile]
+            ).astype(jnp.bfloat16)
         return carry
 
     def loop(step, hooks=(), count=seqs):
@@ -607,8 +616,7 @@
     pass_r(2)
     arrived(2)
     project(2, f_ref, head_lanes(0, 0))
-    loop(paired(lambda s: decays(0, 0, s)), ((twos - 1, lambda: pass_r(3)),), count=twos)
-    pass_y(5)
+    loop(paired(lambda s: decays(0, 0, s)), ((1, lambda: pass_y(5)), (twos - 1, lambda: pass_r(3))), count=twos)
     arrived(3)
     project(3, v_ref, head_lanes(0, 0))
     d_copy(0).wait_recv()
@@ -681,13 +689,12 @@
     time = 293 + 6 * seqs
     arrived(8)
     project(8, g_ref, group_lanes(0))
-    advance(time, 356)
+    advance(time, time + 15)
     arrived(9)
     project(9, g_ref, group_lanes(1))
-    advance(356, 368)
-    lax.fori_loop(reached(0, 368), seqs, chain, 0)
-    done = jnp.where(not_top, total, reached(1, 368))
-    lax.fori_loop(reached(1, 368), done, chain, 0)
+    advance(time + 15, time + 27)
+    lax.fori_loop(reached(0, time + 27), seqs, chain, 0)
+    lax.fori_loop(reached(1, time + 27), total, chain, 0)
     pass_r(10)
     pass_r(11)
 
@@ -701,11 +708,13 @@
 
     settle(d_send, groups, dsend)
     settle(b_send, total, bs)
-    settle(s_send.at[0], bulk(range(units)))
+    for later, us in enumerate((range(unit_g), range(unit_g, units))):
+        settle(s_send.at[later, 0], bulk(us))
+        for k in range(peers):
+            settle(s_send.at[later, 1 + k], bulk(us))
     for k in range(peers):
         settle(y_send.at[k], bulk((0, 1)) + bulk(z_units, True))
         settle(r_send.at[0, k], bulk((0, 1)))
-        settle(s_send.at[1 + k], bulk(range(units)))
 
         @pl.when(not_base)
         def _():
@@ -723,10 +732,6 @@
     arrived(11)
 
     def ending(t, carry):
-        def goal(t):
-            return jnp.maximum(seqs + jnp.minimum(2 * t + 4, seqs), done)
-
-        lax.fori_loop(jnp.where(t == 0, done, goal(t - 1)), goal(t), chain, 0)
         for g in range(groups):
             for b in range(2):
                 t_copy(g * seqs + 2 * t + b).wait_recv()
@@ -774,8 +779,8 @@
     shapes = [(width, hk)] * 4 + [(width, half)] * (4 * groups - 2) + [(cols, width // 2)] * 2
     out = pl.pallas_call(
         functools.partial(layer_kernel, n, ways, heads, axes),
-        out_shape=pltpu.VMEM((rows, width), f32),
-        in_specs=[pl.BlockSpec(memory_space=pltpu.HBM)] * 11,
+        out_shape=pltpu.VMEM((rows, width), bf16),
+        in_specs=[pl.BlockSpec(memory_space=pltpu.HBM)] * 12,
         out_specs=pl.BlockSpec(memory_space=pltpu.VMEM),
         scratch_shapes=[pltpu.VMEM(shape, bf16) for shape in shapes]
         + [
@@ -785,6 +790,8 @@
             pltpu.VMEM((1, cols), f32),
             pltpu.VMEM(initial_state.shape, f32),
             pltpu.VMEM((1, hv), f32),
+            pltpu.VMEM((1, width), f32),
+            pltpu.VMEM((2 * length, width), f32),
             pltpu.VMEM((rows, width), bf16),
             pltpu.VMEM((rows, cols), bf16),
             pltpu.VMEM((rows, cols), bf16),
@@ -808,12 +815,12 @@
             pltpu.VMEM((total, hv, hk), bf16),
             pltpu.VMEM((2, groups, seqs, hk), f32),
             pltpu.VMEM((groups, seqs, hk), f32),
-            dma((9,)),
+            dma((11,)),
             dma((peers,)),
             dma((units, peers)),
             dma((3, peers)),
             dma((units, peers)),
-            dma((1 + peers,)),
+            dma((2, 1 + peers)),
             dma((units,)),
             dma(()),
             dma((n - 1,)),
@@ -849,8 +856,9 @@
         lower_bound[None, :],
         initial_state,
         norm_gain[None, :],
+        post_gain[None, :],
     )
-    return (out * post_gain).astype(bf16).reshape(seqs, length, width)
+    return out.reshape(seqs, length, width)
 
 
 def solution(mesh):

time: 53.4 us -> 52.2 us (0.978)
  other arithmetic: 1.82 us -> 0 us
  local copies, waits for them, and re-layouts: 0.01 us -> 1.32 us
  Pallas kernels: 51 us -> 50.2 us
    convert_element_type x1 -> x0, other arithmetic: 1.82 us -> none  [body(): return (out * post_gain).astype(bf16).reshape(seqs, length, width)]
    unnamed x2 -> x1, local copies, waits for them, and re-layouts: 0.01 us -> 1.32 us
    pallas_call x1, Pallas kernels: 51 us -> 50.2 us  [body(): pl.pallas_call(functools.partial(layer_kernel, n, ways, heads, axes), out...]
where the time goes in v4:
time: 52.2 us; the launch traced here: 51.5 us
  Pallas kernels  50.2 us (96%)
  local copies, waits for them, and re-layouts  1.32 us (3%)
    pallas_call x1, Pallas kernels, body(): pl.pallas_call(functools.partial(layer_kernel, n, ways, heads, axes), out...  50.2 us
    unnamed x1, local copies, waits for them, and re-layouts  1.32 us

profile of v4, /device:TPU:26, one launch (start us, length us, event | category | flops | bytes accessed | tf_op | source)
XLA Modules:
  0.0 51.5 jit_solution(436031383650967537)
XLA Ops:
  0.0 50.2 %shard_map.118 = bf16[512,2048]{1,0:T(8,128)(2,1)S(1)} custom-call(bf16[8,64,2048]{2,1,0:T(8,128)(2,1)} %tokens_hbm.1, f32[1,2048]{1,0:T(1,128)} %bitcast.6, bf16[512,512]{1,0:T(8,128)(2,1)} %wf_hbm.1, bf16[512,512]{1,0:T(8,128)(2,1)} %wv_hbm.1, bf16[512,512]{1,0:T(8,128)(2,1)} %wq_hbm.1, bf16[512,512]{1,0:T(8,128)(2,1)} %wg_hbm.1, ...), custom_call_target="tpu_custom_call" | custom-call | flops 6000000000 | bytes 20000000 | tf_op jit(solution)/shard_map/pallas_call | solution.py:780
  50.2 1.3 %copy.14 = bf16[8,64,2048]{2,1,0:T(8,128)(2,1)} copy(bf16[8,64,2048]{2,1,0:T(8,128)(2,1)S(1)} %bitcast.5) | data formatting | bytes 4194304
